TPU v7x, 256 devices: a whole 4x4x8 slice. The times are simulated.
256 devices in a mesh: ep: 64 (over z, y, core), tp: 4 (over x).
Axes of the slice: x: 4, y: 4, z: 8, core: 2. Of those that a mesh axis runs over, the one named last changes fastest.
Arguments:
- conv_value: bfloat16 [24576, 2048], P('ep', 'tp'), may hold values from -36 to 36
- conv_gate: bfloat16 [24576, 2048], P('ep', 'tp'), may hold values from -8 to 8
- conv_taps: bfloat16 [31, 2048], P(None, 'tp'), may hold values from -1 to 1
- conv_gain: float32 [2048], P('tp'), may hold values from 0.1 to 1.9
- conv_proj: bfloat16 [2048, 2048], P('tp'), may hold values from -0.125 to 0.125
- moe_tokens: bfloat16 [24576, 2048], P('ep'), may hold values from -6 to 6
- moe_gain: float32 [2048], replicated, may hold values from 0.1 to 1.9
- routes: int32 [24576, 2], P('ep'), may hold values from 0 to 63, all different within a row; in each aligned block of 384 rows (0 to 383, 384 to 767, ...) at most 18 rows name the same one
- route_weights: float32 [24576, 2], P('ep'), may hold values from 0.3 to 3
- expert_gate: bfloat16 [64, 2048, 1024], P('ep', None, 'tp'), may hold values from -0.125 to 0.125
- expert_up: bfloat16 [64, 2048, 1024], P('ep', None, 'tp'), may hold values from -0.125 to 0.125
- expert_down: bfloat16 [64, 1024, 2048], P('ep', 'tp'), may hold values from -0.1875 to 0.1875
- shared_gate: bfloat16 [2048, 256], replicated, may hold values from -0.125 to 0.125
- shared_up: bfloat16 [2048, 256], replicated, may hold values from -0.125 to 0.125
- shared_down: bfloat16 [256, 2048], P(None, 'tp'), may hold values from -0.375 to 0.375
Outputs:
- conv_result: bfloat16 [24576, 2048], P('ep', 'tp')
- moe_result: bfloat16 [24576, 2048], P('ep', 'tp')
Inputs may be any that keep to these rules, and one draw needn't show every extreme that they name: `routes`: each row names 2 different experts. Among the 384 rows of one index of ep (aligned blocks in order) no expert is named more than 18 times, and in some blocks one expert is named exactly 18 times.
All inputs are finite; a program needn't handle non-finite values.
Results may differ from a plain program's by a relative error of at most 0.01.
Values may be sent and summed in bfloat16 or wider, within the bound.
A program may use at most 64 MiB of HBM per device.

v0:
```python
import jax
import jax.numpy as jnp
from jax import lax
from jax.sharding import PartitionSpec as P

epsilon = 1e-05


def passed_along(value, axis, by):
    devices = lax.axis_size(axis)
    pairs = [(i, i + by) for i in range(devices) if 0 <= i + by < devices]
    return lax.ppermute(value, axis, pairs)


def total_of_pieces(value, axis):
    parts = lax.all_gather(value, axis)
    return parts.sum(axis=0)


def shared_hidden_rows(rows, shared_gate, shared_up):
    return (
        jax.nn.silu(jnp.dot(rows, shared_gate, preferred_element_type=jnp.float32))
        * jnp.dot(rows, shared_up, preferred_element_type=jnp.float32)
    ).astype(jnp.bfloat16)


def local(
    conv_value,
    conv_gate,
    conv_taps,
    conv_gain,
    conv_proj,
    moe_tokens,
    moe_gain,
    routes,
    route_weights,
    expert_gate,
    expert_up,
    expert_down,
    shared_gate,
    shared_up,
    shared_down,
):
    model_width = moe_tokens.shape[1]
    tok_rows = conv_value.shape[0]
    kernel = conv_taps.shape[0]
    gated_rows = (
        conv_value.astype(jnp.float32) * jax.nn.sigmoid(conv_gate.astype(jnp.float32))
    ).astype(jnp.bfloat16)
    previous = passed_along(gated_rows[tok_rows - (kernel - 1) :], "ep", 1)
    padded = jnp.concatenate([previous, gated_rows], axis=0).astype(jnp.float32)
    tap_weights = conv_taps.astype(jnp.float32)
    convolved = jnp.zeros(gated_rows.shape, jnp.float32)
    for offset in range(kernel):
        convolved = convolved + tap_weights[offset][None, :] * padded[offset : offset + tok_rows]
    total_sum, square_sum = (
        total_of_pieces(jnp.sum(convolved, axis=1), "tp"),
        total_of_pieces(jnp.sum(convolved * convolved, axis=1), "tp"),
    )
    average = total_sum / model_width
    variance = square_sum / model_width - average * average
    scaled = (
        (convolved - average[:, None]) * lax.rsqrt(variance + epsilon)[:, None] * conv_gain[None, :]
    )
    activated = jax.nn.silu(scaled).astype(jnp.bfloat16)
    conv_partial = jnp.dot(activated, conv_proj, preferred_element_type=jnp.float32)
    tokens = moe_tokens.astype(jnp.float32)
    token_mean = jnp.mean(tokens, axis=1, keepdims=True)
    centered = tokens - token_mean
    token_var = jnp.mean(centered * centered, axis=1, keepdims=True)
    normalized = (centered * lax.rsqrt(token_var + epsilon) * moe_gain[None, :]).astype(
        jnp.bfloat16
    )
    shared_hidden = shared_hidden_rows(normalized, shared_gate, shared_up)
    shared_part = jnp.dot(shared_hidden, shared_down, preferred_element_type=jnp.float32)
    experts = lax.axis_size("ep")
    top_count = routes.shape[1]
    capacity = 3 * tok_rows * top_count // (2 * experts)
    entries = tok_rows * top_count
    flat_routes = routes.reshape(-1)
    one_hot = (flat_routes[:, None] == jnp.arange(experts, dtype=jnp.int32)[None, :]).astype(
        jnp.int32
    )
    before = jnp.cumsum(one_hot, axis=0) - one_hot
    slot_rank = jnp.sum(before * one_hot, axis=1)
    slot_index = flat_routes * capacity + slot_rank
    source_row = (
        jnp.full((experts * capacity,), -1, jnp.int32)
        .at[slot_index]
        .set(jnp.arange(entries, dtype=jnp.int32))
    )
    filled = source_row >= 0
    token_index = jnp.where(filled, source_row // top_count, 0)
    outgoing = jnp.where(filled[:, None], normalized[token_index], jnp.zeros((), jnp.bfloat16))
    outgoing = outgoing.reshape(experts, capacity, model_width)
    quarter = model_width // lax.axis_size("tp")
    first_column = lax.axis_index("tp") * quarter
    column_block = lax.dynamic_slice_in_dim(outgoing, first_column, quarter, 2)
    arrived = lax.all_to_all(column_block, "ep", split_axis=0, concat_axis=0, tiled=True)
    arrived = lax.all_gather(arrived, "tp", axis=2, tiled=True)
    expert_input = arrived.reshape(experts * capacity, model_width)
    hidden = (
        jax.nn.silu(jnp.dot(expert_input, expert_gate[0], preferred_element_type=jnp.float32))
        * jnp.dot(expert_input, expert_up[0], preferred_element_type=jnp.float32)
    ).astype(jnp.bfloat16)
    expert_partial = jnp.dot(hidden, expert_down[0], preferred_element_type=jnp.float32)
    conv_sum, expert_sum = (
        lax.psum_scatter(
            conv_partial.astype(jnp.bfloat16), "tp", scatter_dimension=1, tiled=True
        ).astype(jnp.float32),
        lax.psum_scatter(
            expert_partial.astype(jnp.bfloat16), "tp", scatter_dimension=1, tiled=True
        ).astype(jnp.float32),
    )
    conv_result = conv_sum.astype(jnp.bfloat16)
    expert_rows = expert_sum.astype(jnp.bfloat16).reshape(experts, capacity, expert_sum.shape[1])
    returned = lax.all_to_all(expert_rows, "ep", split_axis=0, concat_axis=0, tiled=True)
    picked = returned.reshape(experts * capacity, returned.shape[2])[slot_index]
    picked = picked.astype(jnp.float32).reshape(tok_rows, top_count, returned.shape[2])
    moe_result = (shared_part + jnp.sum(route_weights[:, :, None] * picked, axis=1)).astype(
        jnp.bfloat16
    )
    return (conv_result, moe_result)


def solution(mesh):
    placed = (
        P("ep", "tp"),
        P("ep", "tp"),
        P(None, "tp"),
        P("tp"),
        P("tp", None),
        P("ep", None),
        P(),
        P("ep", None),
        P("ep", None),
        P("ep", None, "tp"),
        P("ep", None, "tp"),
        P("ep", "tp", None),
        P(),
        P(),
        P(None, "tp"),
    )
    return jax.shard_map(
        local, mesh=mesh, in_specs=placed, out_specs=(P("ep", "tp"), P("ep", "tp")), check_vma=False
    )
```

profile of v0, /device:TPU:1, one launch (start us, length us, event | category | flops | bytes accessed | tf_op | source)
XLA Modules:
  0.0 311.6 jit_solution(3662823600982574159)
XLA Ops:
  7.2 0.0 copy-start
  7.2 0.0 all-gather.6.cloned.1.call-start
  7.2 1.0 copy.25
  8.2 0.1 eq.29
  8.3 0.1 eq.25
  8.5 0.7 broadcast_multiply_fusion
  9.2 1.8 reduce-window.6
  11.0 0.3 slice_reduce_fusion
  11.3 0.1 copy.24
  11.4 0.2 mul.517
  11.6 0.1 fusion.60
  11.8 3.4 %scatter_custom_fusion = s32[1152]{0:T(1024)S(1)} fusion(s32[768]{0:T(1024)S(1)} %fusion.68, s32[768]{0:T(1024)S(1)} %iota.11, s32[]{:T(128)} %constant.26.clone.1), kind=kCustom, calls=%fused_computation.127 | custom fusion | bytes 4612 | tf_op jit(solution)/shard_map/scatter | solution.py:90
  15.2 0.0 copy-start.1
  15.2 0.0 copy-start.5
  15.2 1.8 convert_reduce_fusion
  17.1 0.0 copy-done.1
  17.1 0.6 fusion.2
  17.6 0.0 copy-done.5
  17.6 1.7 fusion.4
  19.3 12.3 %gather_fusion = bf16[1152,2048]{1,0:T(8,128)(2,1)} fusion(bf16[384,2048]{1,0:T(8,128)(2,1)} %fusion.4, s32[2048]{0:T(1024)S(1)} %pad_clamp_fusion), kind=kCustom, calls=%fused_computation | custom fusion | bytes 9441792 | tf_op jit(solution)/shard_map/gather | solution.py:94
  31.6 7.6 %gather.9 = bf16[64,18,2048]{2,1,0:T(8,128)(2,1)} reshape(bf16[1152,2048]{1,0:T(8,128)(2,1)} %gather_fusion) | data formatting | bytes 9437184 | tf_op jit(solution)/shard_map/gather | solution.py:94
  39.2 0.1 broadcast_in_dim.21
  39.3 1.8 dynamic-slice_select_fusion
  41.2 52.1 %all_to_all.10 = bf16[64,18,512]{2,1,0:T(8,128)(2,1)} all-to-all(bf16[64,18,512]{2,1,0:T(8,128)(2,1)S(1)} %dynamic-slice_select_fusion), channel_id=1, replica_groups=mesh['ep'=64,'tp'=4] {'ep'}, dimensions={0} | all-to-all | bytes 2359296 | tf_op jit(solution)/shard_map/all_to_all | solution.py:99
  93.3 0.0 all-gather.6.cloned.1.call-update
  93.3 0.2 reduce-scatter.5.cloned.1.call-start
  93.5 64.9 %all-gather.6.cloned.1.call-done = bf16[64,18,2048]{2,1,0:T(8,128)(2,1)} async-done(((bf16[64,18,512]{2,1,0:T(8,128)(2,1)}), bf16[64,18,2048]{2,1,0:T(8,128)(2,1)}) %all-gather.6.cloned.1.call-update) | async-done | bytes 4718608 | tf_op jit(solution)/shard_map/all_gather | solution.py:100
  158.5 7.8 %reshape.99 = bf16[1152,2048]{1,0:T(8,128)(2,1)} reshape(bf16[64,18,2048]{2,1,0:T(8,128)(2,1)} %all-gather.6.cloned.1.call-done) | data formatting | bytes 9437184 | tf_op jit(solution)/shard_map/reshape | solution.py:101
  166.2 5.1 %fusion.16 = f32[1152,256]{1,0:T(8,128)} fusion(bf16[1152,2048]{1,0:T(8,128)(2,1)} %reshape.99, bf16[1,2048,256]{2,1,0:T(8,128)(2,1)} %param.24), kind=kOutput, calls=%fused_computation.27 | convolution fusion | flops 1207959552 | bytes 6946816 | tf_op jit(solution)/shard_map/dot_general | solution.py:103
  171.3 10.3 %convolution_convert_fusion = bf16[1152,2048]{1,0:T(8,128)(2,1)} fusion(bf16[1152,2048]{1,0:T(8,128)(2,1)} %reshape.99, f32[1152,256]{1,0:T(8,128)} %fusion.16, bf16[1,256,2048]{2,1,0:T(8,128)(2,1)} %param.26, bf16[1,2048,256]{2,1,0:T(8,128)(2,1)} %param.25), kind=kOutput, calls=%fused_computation.3 | convolution fusion | flops 2420047872 | bytes 12713984 | tf_op jit(solution)/shard_map/dot_general | solution.py:106
  181.6 0.0 copy-start.2
  181.6 0.0 copy-start.3
  181.6 0.0 copy-start.4
  181.6 0.0 reduce-scatter.5.cloned.1.call-update
  181.6 0.0 reduce-scatter.3.cloned.1.call-start
  181.7 0.9 copy-done.2
  182.6 0.1 copy-done.3
  182.7 0.2 multiply_convert_fusion.1
  182.9 3.8 %collective-permute-start = (bf16[30,512]{1,0:T(8,128)(2,1)S(1)}, bf16[30,512]{1,0:T(8,128)(2,1)S(1)}, u32[]{:S(2)}, u32[]{:S(2)}) collective-permute-start(bf16[30,512]{1,0:T(8,128)(2,1)S(1)} %slice.265), channel_id=1, source_target_pairs={{0,4},{4,8},{8,12},{12,16},{16,20},{20,24},{24,28},{28,32},{32,36}... | collective-permute-start | bytes 92168 | tf_op jit(solution)/shard_map/ppermute | solution.py:12
  186.8 0.0 copy-done.4
  186.9 0.9 collective-permute-done
  187.8 0.1 maximum_convert_fusion
  187.9 0.0 copy-start.8
  187.9 3.8 %fusion.72 = (f32[384]{0:T(512)S(1)}, f32[384]{0:T(512)S(1)}, f32[384,512]{1,0:T(8,128)S(1)}) fusion(f32[414,512]{1,0:T(8,128)S(1)} %maximum_convert_fusion, f32[512]{0:T(512)S(1)} %bitcast.100, f32[512]{0:T(512)S(1)} %bitcast.99, f32[512]{0:T(512)S(1)} %bitcast.98, f32[512]{0:T(512)S(1)} %bitcast.97, f32[512]{0:T(512)S(1)} %bitcast.96, ...), kind=kLoop, calls=%fused_computation.138 | loop fusion | flops 12582144 | bytes 25232384 | tf_op jit(solution)/shard_map/reduce_sum | solution.py:57
  191.8 9.1 %all-gather.2 = f32[4,1,384]{2,1,0:T(1,128)S(1)} all-gather(f32[1,1,384]{2,1,0:T(1,128)S(1)} %reshape.130), channel_id=2, replica_groups=mesh['ep'=64,'tp'=4] {'tp'}, dimensions={0}, use_global_device_ids=true | all-gather | bytes 7680 | tf_op jit(solution)/shard_map/all_gather | solution.py:16
  200.9 9.6 %all-gather.3 = f32[4,1,384]{2,1,0:T(1,128)S(1)} all-gather(f32[1,1,384]{2,1,0:T(1,128)S(1)} %reshape.132), channel_id=3, replica_groups=mesh['ep'=64,'tp'=4] {'tp'}, dimensions={0}, use_global_device_ids=true | all-gather | bytes 7680 | tf_op jit(solution)/shard_map/all_gather | solution.py:16
  210.5 0.0 copy-done
  210.5 0.0 copy-done.8
  210.5 2.3 convolution_convert_fusion.1
  212.8 0.0 reduce-scatter.3.cloned.1.call-update
  212.9 23.5 %reduce-scatter.5.cloned.1.call-done = bf16[1152,512]{1,0:T(8,128)(2,1)} async-done(((bf16[1152,2048]{1,0:T(8,128)(2,1)}), bf16[1152,512]{1,0:T(8,128)(2,1)}) %reduce-scatter.5.cloned.1.call-update) | async-done | bytes 1179664 | tf_op jit(solution)/shard_map/reduce_scatter | solution.py:111
  236.4 3.0 reshape.100
  239.4 0.0 copy-start.6
  239.4 11.1 %all-to-all-start.1 = ((bf16[64,18,512]{2,1,0:T(8,128)(2,1)}), bf16[64,18,512]{2,1,0:T(8,128)(2,1)}, u32[]{:S(2)}, u32[]{:S(2)}) async-start(bf16[64,18,512]{2,1,0:T(8,128)(2,1)} %reshape.100), calls=%async_computation.3 | async-start | bytes 3145728 | tf_op jit(solution)/shard_map/all_to_all | solution.py:117
  250.5 0.0 copy-done.6
  250.5 0.1 copy.23
  250.7 3.1 fusion.76
  253.7 35.8 %all-to-all-done.1 = bf16[64,18,512]{2,1,0:T(8,128)(2,1)} async-done(((bf16[64,18,512]{2,1,0:T(8,128)(2,1)}), bf16[64,18,512]{2,1,0:T(8,128)(2,1)}, u32[]{:S(2)}, u32[]{:S(2)}) %all-to-all-start.1) | async-done | bytes 1179680 | tf_op jit(solution)/shard_map/all_to_all | solution.py:117
  289.5 2.3 reshape.101
  291.8 3.3 %gather_fusion.1 = bf16[768,512]{1,0:T(8,128)(2,1)} fusion(bf16[1152,512]{1,0:T(8,128)(2,1)S(1)} %reshape.101, s32[1024]{0:T(1024)S(1)} %pad_clamp_fusion.1), kind=kCustom, calls=%fused_computation.1 | custom fusion | bytes 1575936 | tf_op jit(solution)/shard_map/gather | solution.py:118
  295.1 3.0 reshape.102
  298.1 3.6 %multiply_reduce_fusion = f32[384,512]{1,0:T(8,128)S(1)} fusion(f32[384,2,512]{2,1,0:T(2,128)} %reshape.102, f32[384,2]{1,0:T(8,128)S(1)} %copy.23), kind=kLoop, calls=%fused_computation.15 | loop fusion | flops 589824 | bytes 2362368 | tf_op jit(solution)/shard_map/reduce_sum | solution.py:120
  301.7 0.0 copy-done.7
  301.7 3.4 %fusion.6 = bf16[384,512]{1,0:T(8,128)(2,1)} fusion(f32[384,512]{1,0:T(8,128)S(1)} %multiply_reduce_fusion, bf16[256,512]{1,0:T(8,128)(2,1)S(1)} %copy-done.7, bf16[384,2048]{1,0:T(8,128)(2,1)} %fusion.4, bf16[2048,256]{1,0:T(8,128)(2,1)} %param.28, f32[384,256]{1,0:T(8,128)} %fusion.76), kind=kOutput, calls=%fused_computation.17 | convolution fusion | flops 504299520 | bytes 4456448 | tf_op jit(solution)/shard_map/dot_general | solution.py:75
  (20 shorter events, 0.2 us)
Async XLA Ops:
  7.2 203.3 %copy-start = (bf16[512,2048]{1,0:T(8,128)(2,1)S(1)}, bf16[512,2048]{1,0:T(8,128)(2,1)}, u32[]{:S(2)}) copy-start(bf16[512,2048]{1,0:T(8,128)(2,1)} %param.19) | copy-start | bytes 6291460
  7.2 151.3 %all-gather.6.cloned.1.call-start = ((), (), s32[]{:S(2)}) async-start(), calls=%async_computation.5 | async-start | bytes 7864320 | tf_op jit(solution)/shard_map/all_gather | solution.py:100
  15.2 1.9 copy-start.1
  15.2 2.4 copy-start.5
  93.3 143.1 %reduce-scatter.5.cloned.1.call-start = ((), (), s32[]{:S(2)}) async-start(), calls=%async_computation.6 | async-start | bytes 5898240 | tf_op jit(solution)/shard_map/reduce_scatter | solution.py:111
  181.6 1.0 copy-start.2
  181.6 1.1 copy-start.3
  181.6 5.2 %copy-start.4 = (bf16[31,512]{1,0:T(8,128)(2,1)S(1)}, bf16[31,512]{1,0:T(8,128)(2,1)}, u32[]{:S(2)}) copy-start(bf16[31,512]{1,0:T(8,128)(2,1)} %param.17) | copy-start | bytes 95236
  181.6 123.5 %reduce-scatter.3.cloned.1.call-start = ((), (), s32[]{:S(2)}) async-start(), calls=%async_computation.4 | async-start | bytes 1966080 | tf_op jit(solution)/shard_map/reduce_scatter | solution.py:108
  182.9 4.9 %collective-permute-start = (bf16[30,512]{1,0:T(8,128)(2,1)S(1)}, bf16[30,512]{1,0:T(8,128)(2,1)S(1)}, u32[]{:S(2)}, u32[]{:S(2)}) collective-permute-start(bf16[30,512]{1,0:T(8,128)(2,1)S(1)} %slice.265), channel_id=1, source_target_pairs={{0,4},{4,8},{8,12},{12,16},{16,20},{20,24},{24,28},{28,32},{32,36}... | collective-permute-start | bytes 92168 | tf_op jit(solution)/shard_map/ppermute | solution.py:12
  187.9 22.6 %copy-start.8 = (f32[512]{0:T(512)S(1)}, f32[512]{0:T(512)}, u32[]{:S(2)}) copy-start(f32[512]{0:T(512)} %param.18) | copy-start | bytes 6148
  239.4 11.1 %copy-start.6 = (f32[384,2]{0,1:T(2,128)S(1)}, f32[384,2]{0,1:T(2,128)}, u32[]{:S(2)}) copy-start(f32[384,2]{0,1:T(2,128)} %param.23) | copy-start | bytes 9220
  239.4 50.1 %all-to-all-start.1 = ((bf16[64,18,512]{2,1,0:T(8,128)(2,1)}), bf16[64,18,512]{2,1,0:T(8,128)(2,1)}, u32[]{:S(2)}, u32[]{:S(2)}) async-start(bf16[64,18,512]{2,1,0:T(8,128)(2,1)} %reshape.100), calls=%async_computation.3 | async-start | bytes 3145728 | tf_op jit(solution)/shard_map/all_to_all | solution.py:117
  298.1 3.6 %copy-start.7 = (bf16[256,512]{1,0:T(8,128)(2,1)S(1)}, bf16[256,512]{1,0:T(8,128)(2,1)}, u32[]{:S(2)}) copy-start(bf16[256,512]{1,0:T(8,128)(2,1)} %param.29) | copy-start | bytes 786436
Sparse Core Ops, SparseCore 0:
  93.4 65.0 all-gather.5
  181.7 54.6 reduce-scatter.4
  239.5 27.0 reduce-scatter.2
where the time goes:
time: 313 us; the launch traced here: 312 us
  waiting for transfers between devices  125 us (40%)
  blocking collectives  70.7 us (23%)
  local copies, waits for them, and re-layouts  45.9 us (15%)
  matrix products  24.2 us (8%)
  other arithmetic  16.4 us (5%)
  starting transfers between devices  15.2 us (5%)
  between operations  14 us (4%)
    all_gather x1, waiting for transfers between devices, local(): arrived = lax.all_gather(arrived, 'tp', axis=2, tiled=True)  64.9 us
    all_to_all x1, blocking collectives, local(): lax.all_to_all(column_block, 'ep', split_axis=0, concat_axis=0, tiled=True)  52.1 us
    all_to_all x1, waiting for transfers between devices, local(): lax.all_to_all(expert_rows, 'ep', split_axis=0, concat_axis=0, tiled=True)  35.8 us
    reduce_scatter x1, waiting for transfers between devices, local(): lax.psum_scatter(expert_partial.astype(jnp.bfloat16), 'tp', scatter_dimen...  23.5 us
    gather x2, local copies, waits for them, and re-layouts, local(): normalized[token_index]  19.9 us
    all_gather x2, blocking collectives, total_of_pieces(): parts = lax.all_gather(value, axis)  18.6 us
    all_to_all x1, starting transfers between devices, local(): lax.all_to_all(expert_rows, 'ep', split_axis=0, concat_axis=0, tiled=True)  11.1 us
    dot_general x1, matrix products, local(): jnp.dot(hidden, expert_down[0], preferred_element_type=jnp.float32)  10.3 us
  transfers between devices with their start and end apart: 5, of which 4 were waited for; matrix products, arithmetic and copies ran while one was open for 9% of the time, Pallas kernels for 0%

commit v1 on v0

--- a/solution.py
+++ b/solution.py
@@ -97,7 +97,10 @@
     first_column = lax.axis_index("tp") * quarter
     column_block = lax.dynamic_slice_in_dim(outgoing, first_column, quarter, 2)
     arrived = lax.all_to_all(column_block, "ep", split_axis=0, concat_axis=0, tiled=True)
-    arrived = lax.all_gather(arrived, "tp", axis=2, tiled=True)
+    count = lax.axis_size("tp")
+    pieces = jnp.stack([arrived for _ in range(count)])
+    pieces = lax.all_to_all(pieces, "tp", split_axis=0, concat_axis=0)
+    arrived = jnp.concatenate(pieces, axis=2)
     expert_input = arrived.reshape(experts * capacity, model_width)
     hidden = (
         jax.nn.silu(jnp.dot(expert_input, expert_gate[0], preferred_element_type=jnp.float32))

time: 313 us -> 299 us (0.955)
  waiting for transfers between devices: 125 us -> 54.5 us
  blocking collectives: 70.7 us -> 128 us
    all_gather x1 -> x0, waiting for transfers between devices: 64.9 us -> none  [local(): arrived = lax.all_gather(arrived, 'tp', axis=2, tiled=True)]
    all_to_all x0 -> x1, blocking collectives: none -> 56.6 us  [local(): pieces = lax.all_to_all(pieces, 'tp', split_axis=0, concat_axis=0)]
    reduce_scatter x1, waiting for transfers between devices: 23.5 us -> 18 us  [local(): lax.psum_scatter(expert_partial.astype(jnp.bfloat16), 'tp', scatter_dimen...]
    unnamed x22 -> x27, local copies, waits for them, and re-layouts: 2.18 us -> 6.34 us
    reshape x1, local copies, waits for them, and re-layouts: 7.77 us -> 3.64 us  [local(): arrived = jnp.concatenate(pieces, axis=2)]
  transfers between devices with their start and end apart: 5 -> 4, of which waited for: 4 -> 3; matrix products, arithmetic and copies ran while one was open for 9% -> 10% of each run, Pallas kernels for 0% -> 0%
where the time goes in v1:
time: 299 us; the launch traced here: 298 us
  blocking collectives  128 us (43%)
  waiting for transfers between devices  54.5 us (18%)
  local copies, waits for them, and re-layouts  46.9 us (16%)
  matrix products  21.5 us (7%)
  starting transfers between devices  16.4 us (5%)
  other arithmetic  16.4 us (5%)
  between operations  14.4 us (5%)
    all_to_all x1, blocking collectives, local(): pieces = lax.all_to_all(pieces, 'tp', split_axis=0, concat_axis=0)  56.6 us
    all_to_all x1, blocking collectives, local(): lax.all_to_all(column_block, 'ep', split_axis=0, concat_axis=0, tiled=True)  52 us
    all_to_all x1, waiting for transfers between devices, local(): lax.all_to_all(expert_rows, 'ep', split_axis=0, concat_axis=0, tiled=True)  35.8 us
    gather x2, local copies, waits for them, and re-layouts, local(): normalized[token_index]  19.9 us
    all_gather x2, blocking collectives, total_of_pieces(): parts = lax.all_gather(value, axis)  19.2 us
    reduce_scatter x1, waiting for transfers between devices, local(): lax.psum_scatter(expert_partial.astype(jnp.bfloat16), 'tp', scatter_dimen...  18 us
    all_to_all x1, starting transfers between devices, local(): lax.all_to_all(expert_rows, 'ep', split_axis=0, concat_axis=0, tiled=True)  11.1 us
    dot_general x1, matrix products, local(): jnp.dot(hidden, expert_down[0], preferred_element_type=jnp.float32)  10.3 us
  transfers between devices with their start and end apart: 4, of which 3 were waited for; matrix products, arithmetic and copies ran while one was open for 10% of the time, Pallas kernels for 0%

profile of v1, /device:TPU:1, one launch (start us, length us, event | category | flops | bytes accessed | tf_op | source)
XLA Modules:
  0.0 297.8 jit_solution(13687065737893794231)
XLA Ops:
  7.2 0.0 copy-start
  7.2 0.0 reduce-scatter.5.cloned.1.call-start
  7.2 1.0 copy.31
  8.2 0.1 eq.29
  8.3 0.1 eq.25
  8.5 0.7 broadcast_multiply_fusion
  9.2 1.8 reduce-window.6
  11.0 0.3 slice_reduce_fusion
  11.3 0.1 copy.30
  11.4 0.2 mul.517
  11.6 0.1 fusion.60
  11.8 3.4 %scatter_custom_fusion = s32[1152]{0:T(1024)S(1)} fusion(s32[768]{0:T(1024)S(1)} %fusion.68, s32[768]{0:T(1024)S(1)} %iota.11, s32[]{:T(128)} %constant.26.clone.1), kind=kCustom, calls=%fused_computation.127 | custom fusion | bytes 4612 | tf_op jit(solution)/shard_map/scatter | solution.py:90
  15.2 0.0 copy-start.1
  15.2 0.0 copy-start.6
  15.2 1.8 convert_reduce_fusion
  17.1 0.0 copy-done.1
  17.1 0.6 fusion.2
  17.6 0.0 copy-done.6
  17.6 1.7 fusion.4
  19.3 12.3 %gather_fusion = bf16[1152,2048]{1,0:T(8,128)(2,1)} fusion(bf16[384,2048]{1,0:T(8,128)(2,1)} %fusion.4, s32[2048]{0:T(1024)S(1)} %pad_clamp_fusion), kind=kCustom, calls=%fused_computation | custom fusion | bytes 9441792 | tf_op jit(solution)/shard_map/gather | solution.py:94
  31.6 7.6 %gather.9 = bf16[64,18,2048]{2,1,0:T(8,128)(2,1)} reshape(bf16[1152,2048]{1,0:T(8,128)(2,1)} %gather_fusion) | data formatting | bytes 9437184 | tf_op jit(solution)/shard_map/gather | solution.py:94
  39.2 0.1 broadcast_in_dim.21
  39.3 1.8 dynamic-slice_select_fusion
  41.2 52.0 %all_to_all.15 = bf16[64,18,512]{2,1,0:T(8,128)(2,1)S(1)} all-to-all(bf16[64,18,512]{2,1,0:T(8,128)(2,1)S(1)} %dynamic-slice_select_fusion), channel_id=1, replica_groups=mesh['ep'=64,'tp'=4] {'ep'}, dimensions={0} | all-to-all | bytes 2359296 | tf_op jit(solution)/shard_map/all_to_all | solution.py:99
  93.2 0.4 copy.34
  93.5 0.6 stack.2
  94.1 56.6 %all_to_all.16 = bf16[4,64,18,512]{3,1,2,0:T(8,128)(2,1)S(1)} all-to-all(bf16[4,64,18,512]{3,1,2,0:T(8,128)(2,1)S(1)} %stack.2), channel_id=1, replica_groups=mesh['ep'=64,'tp'=4] {'tp'}, dimensions={0} | all-to-all | bytes 9437184 | tf_op jit(solution)/shard_map/all_to_all | solution.py:102
  150.7 3.6 %copy.35 = bf16[64,18,4,512]{3,2,1,0:T(4,128)(2,1)S(1)} copy(bf16[64,18,4,512]{3,0,1,2:T(8,128)(2,1)S(1)} %bitcast.73) | data formatting | bytes 9437184 | tf_op jit(solution)/shard_map/reshape | solution.py:103
  154.3 0.0 copy-start.8
  154.4 2.0 copy.37
  156.4 0.0 copy-start.2
  156.4 2.2 copy-done.2
  158.5 0.0 copy-done.8
  158.5 2.4 fusion.16
  160.9 10.3 %convolution_convert_fusion = bf16[1152,2048]{1,0:T(8,128)(2,1)} fusion(bf16[1152,2048]{1,0:T(8,128)(2,1)} %bitcast.76, f32[1152,256]{1,0:T(8,128)} %fusion.16, bf16[1,256,2048]{2,1,0:T(8,128)(2,1)} %param.26, bf16[1,2048,256]{2,1,0:T(8,128)(2,1)} %param.25), kind=kOutput, calls=%fused_computation.3 | convolution fusion | flops 2420047872 | bytes 12713984 | tf_op jit(solution)/shard_map/dot_general | solution.py:109
  171.2 0.0 reduce-scatter.5.cloned.1.call-update
  171.2 0.0 reduce-scatter.3.cloned.1.call-start
  171.3 0.9 copy-done.3
  172.2 0.1 copy-done.4
  172.3 0.2 multiply_convert_fusion.1
  172.6 5.3 %collective-permute-start = (bf16[30,512]{1,0:T(8,128)(2,1)S(1)}, bf16[30,512]{1,0:T(8,128)(2,1)S(1)}, u32[]{:S(2)}, u32[]{:S(2)}) collective-permute-start(bf16[30,512]{1,0:T(8,128)(2,1)S(1)} %slice.265), channel_id=1, source_target_pairs={{0,4},{4,8},{8,12},{12,16},{16,20},{20,24},{24,28},{28,32},{32,36}... | collective-permute-start | bytes 92168 | tf_op jit(solution)/shard_map/ppermute | solution.py:12
  177.8 0.0 copy-done.5
  177.9 0.7 collective-permute-done
  178.6 0.1 maximum_convert_fusion
  178.7 0.0 copy-start.10
  178.7 3.8 %fusion.72 = (f32[384]{0:T(512)S(1)}, f32[384]{0:T(512)S(1)}, f32[384,512]{1,0:T(8,128)S(1)}) fusion(f32[414,512]{1,0:T(8,128)S(1)} %maximum_convert_fusion, f32[512]{0:T(512)S(1)} %bitcast.108, f32[512]{0:T(512)S(1)} %bitcast.107, f32[512]{0:T(512)S(1)} %bitcast.106, f32[512]{0:T(512)S(1)} %bitcast.105, f32[512]{0:T(512)S(1)} %bitcast.104, ...), kind=kLoop, calls=%fused_computation.138 | loop fusion | flops 12582144 | bytes 25232384 | tf_op jit(solution)/shard_map/reduce_sum | solution.py:57
  182.6 9.6 %all-gather.2 = f32[4,1,384]{2,1,0:T(1,128)S(1)} all-gather(f32[1,1,384]{2,1,0:T(1,128)S(1)} %reshape.132), channel_id=2, replica_groups=mesh['ep'=64,'tp'=4] {'tp'}, dimensions={0}, use_global_device_ids=true | all-gather | bytes 7680 | tf_op jit(solution)/shard_map/all_gather | solution.py:16
  192.2 9.6 %all-gather.3 = f32[4,1,384]{2,1,0:T(1,128)S(1)} all-gather(f32[1,1,384]{2,1,0:T(1,128)S(1)} %reshape.134), channel_id=3, replica_groups=mesh['ep'=64,'tp'=4] {'tp'}, dimensions={0}, use_global_device_ids=true | all-gather | bytes 7680 | tf_op jit(solution)/shard_map/all_gather | solution.py:16
  201.8 0.0 copy-done
  201.8 0.0 copy-done.10
  201.9 2.3 convolution_convert_fusion.1
  204.2 0.0 reduce-scatter.3.cloned.1.call-update
  204.2 18.0 %reduce-scatter.5.cloned.1.call-done = bf16[1152,512]{1,0:T(8,128)(2,1)} async-done(((bf16[1152,2048]{1,0:T(8,128)(2,1)}), bf16[1152,512]{1,0:T(8,128)(2,1)}) %reduce-scatter.5.cloned.1.call-update) | async-done | bytes 1179664 | tf_op jit(solution)/shard_map/reduce_scatter | solution.py:114
  222.2 3.0 %reshape.102 = bf16[64,18,512]{2,1,0:T(8,128)(2,1)} reshape(bf16[1152,512]{1,0:T(8,128)(2,1)} %reduce-scatter.5.cloned.1.call-done) | data formatting | bytes 2359296 | tf_op jit(solution)/shard_map/reshape | solution.py:119
  225.2 11.1 %all-to-all-start.2 = ((bf16[64,18,512]{2,1,0:T(8,128)(2,1)}), bf16[64,18,512]{2,1,0:T(8,128)(2,1)}, u32[]{:S(2)}, u32[]{:S(2)}) async-start(bf16[64,18,512]{2,1,0:T(8,128)(2,1)} %reshape.102), calls=%async_computation.4 | async-start | bytes 3145728 | tf_op jit(solution)/shard_map/all_to_all | solution.py:120
  236.3 0.1 copy.29
  236.4 3.1 %fusion.76 = f32[384,256]{1,0:T(8,128)} fusion(bf16[384,2048]{1,0:T(8,128)(2,1)} %fusion.4, bf16[2048,256]{1,0:T(8,128)(2,1)} %param.27), kind=kOutput, calls=%fused_computation.141 | convolution fusion | flops 402653184 | bytes 3014656 | tf_op jit(solution)/shard_map/dot_general | solution.py:22
  239.5 35.8 %all-to-all-done.2 = bf16[64,18,512]{2,1,0:T(8,128)(2,1)} async-done(((bf16[64,18,512]{2,1,0:T(8,128)(2,1)}), bf16[64,18,512]{2,1,0:T(8,128)(2,1)}, u32[]{:S(2)}, u32[]{:S(2)}) %all-to-all-start.2) | async-done | bytes 1179680 | tf_op jit(solution)/shard_map/all_to_all | solution.py:120
  275.3 2.3 reshape.103
  277.6 3.3 %gather_fusion.1 = bf16[768,512]{1,0:T(8,128)(2,1)} fusion(bf16[1152,512]{1,0:T(8,128)(2,1)S(1)} %reshape.103, s32[1024]{0:T(1024)S(1)} %pad_clamp_fusion.1), kind=kCustom, calls=%fused_computation.1 | custom fusion | bytes 1575936 | tf_op jit(solution)/shard_map/gather | solution.py:121
  280.9 3.0 reshape.104
  283.9 3.6 %multiply_reduce_fusion = f32[384,512]{1,0:T(8,128)S(1)} fusion(f32[384,2,512]{2,1,0:T(2,128)} %reshape.104, f32[384,2]{1,0:T(8,128)S(1)} %copy.29), kind=kLoop, calls=%fused_computation.15 | loop fusion | flops 589824 | bytes 2362368 | tf_op jit(solution)/shard_map/reduce_sum | solution.py:123
  287.5 0.0 copy-done.9
  287.5 3.4 %fusion.6 = bf16[384,512]{1,0:T(8,128)(2,1)} fusion(f32[384,512]{1,0:T(8,128)S(1)} %multiply_reduce_fusion, bf16[256,512]{1,0:T(8,128)(2,1)S(1)} %copy-done.9, bf16[384,2048]{1,0:T(8,128)(2,1)} %fusion.4, bf16[2048,256]{1,0:T(8,128)(2,1)} %param.28, f32[384,256]{1,0:T(8,128)} %fusion.76), kind=kOutput, calls=%fused_computation.17 | convolution fusion | flops 504299520 | bytes 4456448 | tf_op jit(solution)/shard_map/dot_general | solution.py:75
  (25 shorter events, 0.2 us)
Async XLA Ops:
  7.2 194.7 %copy-start = (bf16[512,2048]{1,0:T(8,128)(2,1)S(1)}, bf16[512,2048]{1,0:T(8,128)(2,1)}, u32[]{:S(2)}) copy-start(bf16[512,2048]{1,0:T(8,128)(2,1)} %param.19) | copy-start | bytes 6291460
  7.2 215.0 %reduce-scatter.5.cloned.1.call-start = ((), (), s32[]{:S(2)}) async-start(), calls=%async_computation.6 | async-start | bytes 5898240 | tf_op jit(solution)/shard_map/reduce_scatter | solution.py:114
  15.2 1.9 copy-start.1
  15.2 2.4 copy-start.6
  154.3 4.2 %copy-start.8 = (bf16[1,2048,256]{2,1,0:T(8,128)(2,1)S(1)}, bf16[1,2048,256]{2,1,0:T(8,128)(2,1)}, u32[]{:S(2)}) copy-start(bf16[1,2048,256]{2,1,0:T(8,128)(2,1)} %param.24) | copy-start | bytes 3145732
  156.4 2.2 copy-start.2
  171.2 1.0 copy-start.3
  171.2 1.1 copy-start.4
  171.2 6.6 %copy-start.5 = (bf16[31,512]{1,0:T(8,128)(2,1)S(1)}, bf16[31,512]{1,0:T(8,128)(2,1)}, u32[]{:S(2)}) copy-start(bf16[31,512]{1,0:T(8,128)(2,1)} %param.17) | copy-start | bytes 95236
  171.2 119.7 %reduce-scatter.3.cloned.1.call-start = ((), (), s32[]{:S(2)}) async-start(), calls=%async_computation.5 | async-start | bytes 1966080 | tf_op jit(solution)/shard_map/reduce_scatter | solution.py:111
  172.6 6.0 %collective-permute-start = (bf16[30,512]{1,0:T(8,128)(2,1)S(1)}, bf16[30,512]{1,0:T(8,128)(2,1)S(1)}, u32[]{:S(2)}, u32[]{:S(2)}) collective-permute-start(bf16[30,512]{1,0:T(8,128)(2,1)S(1)} %slice.265), channel_id=1, source_target_pairs={{0,4},{4,8},{8,12},{12,16},{16,20},{20,24},{24,28},{28,32},{32,36}... | collective-permute-start | bytes 92168 | tf_op jit(solution)/shard_map/ppermute | solution.py:12
  178.7 23.1 %copy-start.10 = (f32[512]{0:T(512)S(1)}, f32[512]{0:T(512)}, u32[]{:S(2)}) copy-start(f32[512]{0:T(512)} %param.18) | copy-start | bytes 6148
  225.2 11.1 %copy-start.7 = (f32[384,2]{0,1:T(2,128)S(1)}, f32[384,2]{0,1:T(2,128)}, u32[]{:S(2)}) copy-start(f32[384,2]{0,1:T(2,128)} %param.23) | copy-start | bytes 9220
  225.2 50.1 %all-to-all-start.2 = ((bf16[64,18,512]{2,1,0:T(8,128)(2,1)}), bf16[64,18,512]{2,1,0:T(8,128)(2,1)}, u32[]{:S(2)}, u32[]{:S(2)}) async-start(bf16[64,18,512]{2,1,0:T(8,128)(2,1)} %reshape.102), calls=%async_computation.4 | async-start | bytes 3145728 | tf_op jit(solution)/shard_map/all_to_all | solution.py:120
  283.9 3.6 %copy-start.9 = (bf16[256,512]{1,0:T(8,128)(2,1)S(1)}, bf16[256,512]{1,0:T(8,128)(2,1)}, u32[]{:S(2)}) copy-start(bf16[256,512]{1,0:T(8,128)(2,1)} %param.29) | copy-start | bytes 786436
Sparse Core Ops, SparseCore 0:
  171.4 50.7 reduce-scatter.4
  225.3 26.9 reduce-scatter.2
